TPU v7x, 32 devices: a whole 2x2x4 slice. The times are simulated.
32 devices in a mesh: rep: 4 (over z), fs: 4 (over y, x), tp: 2 (over core).
Axes of the slice: x: 2, y: 2, z: 4, core: 2. Of those that a mesh axis runs over, the one named last changes fastest.
Arguments:
- tokens_in: bfloat16 [8192, 2048], P(('rep', 'fs', 'tp')), may hold values from -6 to 6
- norm_gain: float32 [2048], replicated, may hold values from 0.1 to 1.9
- gate_weight: bfloat16 [2048, 3072], P(None, ('fs', 'tp')), may hold values from -0.125 to 0.125
- up_weight: bfloat16 [2048, 3072], P(None, ('fs', 'tp')), may hold values from -0.125 to 0.125
- down_weight: bfloat16 [3072, 2048], P(('fs', 'tp')), may hold values from -0.109375 to 0.109375
- out_grad: bfloat16 [8192, 2048], P(('rep', 'fs', 'tp')), may hold values from -6 to 6
Outputs:
- grad_in: bfloat16 [8192, 2048], P(('rep', 'fs', 'tp'))
- grad_gain: float32 [2048], replicated
- grad_gate: float32 [2048, 3072], P(None, ('fs', 'tp'))
- grad_up: float32 [2048, 3072], P(None, ('fs', 'tp'))
- grad_down: float32 [3072, 2048], P(('fs', 'tp'))
All inputs are finite; a program needn't handle non-finite values.
Results may differ from a plain program's by a relative error of at most 0.014.
Values may be sent and summed in bfloat16 or wider, within the bound.
A program may use at most 192 MiB of HBM per device.

v0:
```python
import jax
import jax.numpy as jnp
from jax import lax
from jax.experimental import pallas as pl
from jax.experimental.pallas import tpu as pltpu
from jax.sharding import PartitionSpec as P

norm_eps = 1e-06
MESH = pl.DeviceIdType.MESH
F32, BF16 = jnp.float32, jnp.bfloat16
CHUNKS = 8
NT = (((1,), (1,)), ((), ()))


def flip(f, j):
    return (f % 2 + j % 2) % 2 + 2 * ((f // 2 + j // 2) % 2)


def remote(src, dst, send, recv, dev):
    return pltpu.make_async_remote_copy(
        src_ref=src, dst_ref=dst, send_sem=send, recv_sem=recv, device_id=dev, device_id_type=MESH
    )


def gather_kernel(
    x_ref, g_ref, gain_ref, gw_ref, uw_ref, dw_ref,
    normed_out, grad_out, hid_out, ggp_out, gup_out,
    xall, gall, normed, hid, ggp, gup, ssem, rsem, osem,
):
    f, t = lax.axis_index("fs"), lax.axis_index("tp")
    other = 1 - t
    rows = x_ref.shape[0]
    half = rows // 2
    to_a, to_b, to_p = {"fs": flip(f, 1)}, {"fs": flip(f, 2)}, {"tp": other}
    barrier = pltpu.get_barrier_semaphore()
    for dev in (to_a, to_b, to_p):
        pl.semaphore_signal(barrier, inc=1, device_id=dev, device_id_type=MESH)
    pl.semaphore_wait(barrier, 3)

    def pos(j, core):
        return flip(f, j) * 2 + core

    bufs = ((x_ref, xall), (g_ref, gall))
    low, high = pl.ds(0, half), pl.ds(half, half)

    def copy(n, kind, incoming=False):
        own, held = bufs[n]
        sems = (ssem.at[n, kind], rsem.at[n, kind])
        mine = pos(0, t)
        if kind == 0:
            return remote(own, held.at[pos(1, t) if incoming else mine], *sems, to_a)
        if kind == 1:
            return remote(own, held.at[pos(2, t) if incoming else mine], *sems, to_b)
        if kind == 2:
            return remote(own, held.at[pos(0, other) if incoming else mine], *sems, to_p)
        if kind == 3:
            slot = held.at[pos(3, t) if incoming else pos(1, t), high]
            return remote(slot, slot, *sems, to_b)
        if kind == 4:
            slot = held.at[pos(3, t) if incoming else pos(2, t), low]
            return remote(slot, slot, *sems, to_a)
        j = {5: 1, 6: 2, 7: 3, 8: 3}[kind]
        slot = held.at[pos(j, other if incoming else t)]
        if kind == 7:
            slot = slot.at[low]
        if kind == 8:
            slot = slot.at[high]
        return remote(slot, slot, *sems, to_p)

    for n in range(2):
        for kind in (0, 1, 2):
            copy(n, kind).start()
    xall[pos(0, t)] = x_ref[...]
    gall[pos(0, t)] = g_ref[...]

    def outs(p):
        return [
            pltpu.make_async_copy(src.at[p], dst.at[p], osem.at[i])
            for i, (src, dst) in enumerate(
                ((normed, normed_out), (gall, grad_out), (hid, hid_out), (ggp, ggp_out), (gup, gup_out))
            )
        ]

    def body(i, carry):
        @pl.when(i == 1)
        def _():
            for n in range(2):
                copy(n, 2, True).wait_recv()

        @pl.when(i == 2)
        def _():
            for n in range(2):
                copy(n, 0, True).wait_recv()
                copy(n, 3).start()
                copy(n, 5).start()
                copy(n, 1, True).wait_recv()
                copy(n, 4).start()
                copy(n, 6).start()

        @pl.when(i == 3)
        def _():
            for n in range(2):
                copy(n, 5, True).wait_recv()

        @pl.when(i == 5)
        def _():
            for n in range(2):
                copy(n, 6, True).wait_recv()

        @pl.when(i == 6)
        def _():
            for n in range(2):
                copy(n, 4, True).wait_recv()
                copy(n, 7).start()
                copy(n, 3, True).wait_recv()
                copy(n, 8).start()

        @pl.when(i == 7)
        def _():
            for n in range(2):
                copy(n, 7, True).wait_recv()
                copy(n, 8, True).wait_recv()

        p = flip(f, i // 2) * 2 + (t + i) % 2
        floats = xall[p].astype(F32)
        inverse = lax.rsqrt(jnp.mean(floats * floats, axis=-1, keepdims=True) + norm_eps)
        normed[p] = (floats * inverse * gain_ref[...]).astype(BF16)
        gate_pre = jnp.dot(normed[p], gw_ref[...], preferred_element_type=F32)
        up_pre = jnp.dot(normed[p], uw_ref[...], preferred_element_type=F32)
        grad_hidden = 0.5 * lax.dot_general(gall[p], dw_ref[...], NT, preferred_element_type=F32)
        sigma = jax.nn.sigmoid(gate_pre)
        active = gate_pre * sigma
        hid[p] = (active * up_pre).astype(BF16)
        ggp[p] = (grad_hidden * up_pre * sigma * (1.0 + gate_pre * (1.0 - sigma))).astype(BF16)
        gup[p] = (grad_hidden * active).astype(BF16)
        return carry

    lax.fori_loop(0, 8, body, 0)
    whole = [
        pltpu.make_async_copy(src, dst, osem.at[i])
        for i, (src, dst) in enumerate(
            ((normed, normed_out), (gall, grad_out), (hid, hid_out), (ggp, ggp_out), (gup, gup_out))
        )
    ]
    for c in whole:
        c.start()
    for n in range(2):
        for kind in range(9):
            copy(n, kind).wait_send()
    for c in whole:
        c.wait()


def exit_kernel(
    reps,
    ggp_ref, gup_ref, gw_ref, uw_ref, wd_ref, wg_ref, wu_ref,
    gn_ref, fd_ref, fg_ref, fu_ref,
    ind, ing, inu, tbuf, pin, sbuf, rsin,
    up_send, in_recv, fin_recv, down_send, p_send, p_recv, s_send, s_recv,
):
    f, t, r = lax.axis_index("fs"), lax.axis_index("tp"), lax.axis_index("rep")
    other = 1 - t
    middle = reps // 2
    sign = 1 - 2 * (r // middle)
    up, down = {"rep": r + sign}, {"rep": (r - sign + reps) % reps}
    right = r // middle
    depth = (1 - right) * (middle - 1 - r) + right * (r - middle)
    center, outer = depth == 0, depth == middle - 1
    inner, has_down = depth > 0, depth < middle - 1
    peers = [{"fs": flip(f, 1)}, {"fs": flip(f, 2)}, {"fs": flip(f, 3)}, {"tp": other}, up]
    barrier = pltpu.get_barrier_semaphore()
    for dev in peers:
        pl.semaphore_signal(barrier, inc=1, device_id=dev, device_id_type=MESH)

    @pl.when(has_down)
    def _():
        pl.semaphore_signal(barrier, inc=1, device_id=down, device_id_type=MESH)
        pl.semaphore_wait(barrier, 6)

    @pl.when(outer)
    def _():
        pl.semaphore_wait(barrier, 5)

    arrays = ((wd_ref, ind, fd_ref), (wg_ref, ing, fg_ref), (wu_ref, inu, fu_ref))
    rows = gn_ref.shape[0]
    width = gw_ref.shape[0]
    tile = min(512, width)

    def at(ref, s):
        step = ref.shape[0] // CHUNKS
        return ref.at[pl.ds(pl.multiple_of(s * step, step), step)]

    def up_copy(a, s, src, dst, recv):
        return remote(at(src, s), at(dst, s), up_send.at[a, s], recv.at[a, s], up)

    def down_copy(a, s):
        fin = arrays[a][2]
        return remote(at(fin, s), at(fin, s), down_send.at[a, s], fin_recv.at[a, s], down)

    @pl.when(outer)
    def _():
        def first(s, carry):
            for a, (own, inc, fin) in enumerate(arrays):
                up_copy(a, s, own, inc, in_recv).start()
            return carry

        lax.fori_loop(0, CHUNKS, first, 0)

    def pair_copy(j):
        return remote(tbuf.at[j], pin.at[j], p_send.at[j], p_recv.at[j], {"tp": other})

    def peer_copy(j):
        return remote(sbuf.at[j], rsin.at[j], s_send.at[j], s_recv.at[j], {"fs": flip(f, j)})

    def term(owner, c):
        here = pl.ds(pl.multiple_of(owner * rows, rows), rows)
        cols = pl.ds(pl.multiple_of(c * tile, tile), tile)
        out = lax.dot_general(ggp_ref[here, :], gw_ref[cols, :], NT, preferred_element_type=F32)
        out = out + lax.dot_general(gup_ref[here, :], uw_ref[cols, :], NT, preferred_element_type=F32)
        return out.astype(BF16), cols

    def body(s, carry):
        j = 3 - s % 4

        @pl.when(s < 4)
        def _():
            def one(c, carry):
                value, cols = term(flip(f, j) * 2 + other, c)
                tbuf[j, :, cols] = value
                return carry

            lax.fori_loop(0, width // tile, one, 0)
            pair_copy(j).start()

        @pl.when((s >= 4) & (s < 8))
        def _():
            pair_copy(j).wait_recv()

            def one(c, carry):
                value, cols = term(flip(f, j) * 2 + t, c)
                total = value.astype(F32) + pin[j, :, cols].astype(F32)
                gn_ref[:, cols] = total
                sbuf[j, :, cols] = total.astype(BF16)
                return carry

            lax.fori_loop(0, width // tile, one, 0)

            @pl.when(j > 0)
            def _():
                peer_copy(j).start()

        @pl.when((s < CHUNKS) & has_down)
        def _():
            for a, (own, inc, fin) in enumerate(arrays):
                up_copy(a, s, inc, inc, in_recv).wait_recv()
                here = at(inc, s)
                here[...] = (at(own, s)[...].astype(F32) + here[...].astype(F32)).astype(BF16)

                @pl.when(center)
                def _():
                    up_copy(a, s, inc, fin, fin_recv).start()

                @pl.when(inner)
                def _():
                    up_copy(a, s, inc, inc, in_recv).start()

        @pl.when(s >= 1)
        def _():
            for a, (own, inc, fin) in enumerate(arrays):
                before = s - 1
                down_copy(a, before).wait_recv()

                @pl.when(center)
                def _():
                    here = at(fin, before)
                    here[...] = (at(inc, before)[...].astype(F32) + here[...].astype(F32)).astype(BF16)

                @pl.when(has_down)
                def _():
                    down_copy(a, before).start()

        return carry

    lax.fori_loop(0, CHUNKS + 1, body, 0)
    for j in (3, 2, 1):
        peer_copy(j).wait_recv()
    gn_ref[...] = gn_ref[...] + rsin[3].astype(F32) + rsin[2].astype(F32) + rsin[1].astype(F32)
    for j in (3, 2, 1):
        peer_copy(j).wait_send()
    for j in range(4):
        pair_copy(j).wait_send()

    def last(s, carry):
        for a, (own, inc, fin) in enumerate(arrays):
            up_copy(a, s, own, inc, in_recv).wait_send()

            @pl.when(has_down)
            def _():
                down_copy(a, s).wait_send()

        return carry

    lax.fori_loop(0, CHUNKS, last, 0)


def shards(tokens_in, norm_gain, gate_weight, up_weight, down_weight, out_grad):
    rows, d = tokens_in.shape
    ff = gate_weight.shape[1]
    reps = lax.axis_size("rep")
    ranks = lax.axis_size("fs") * lax.axis_size("tp")
    factor = float(rows * reps * ranks) ** (-0.5)
    vmem, anywhere = pl.BlockSpec(memory_space=pltpu.VMEM), pl.BlockSpec(memory_space=pl.ANY)
    wide, narrow = (ranks, rows, d), (ranks, rows, ff)
    dma = pltpu.SemaphoreType.DMA
    flat = (ranks * rows,)
    gathered = pl.pallas_call(
        gather_kernel,
        out_shape=[jax.ShapeDtypeStruct(s, BF16) for s in (wide, wide, narrow, narrow, narrow)],
        in_specs=[vmem] * 6,
        out_specs=[anywhere] * 5,
        scratch_shapes=[
            pltpu.VMEM(wide, BF16), pltpu.VMEM(wide, BF16), pltpu.VMEM(wide, BF16),
            pltpu.VMEM(narrow, BF16), pltpu.VMEM(narrow, BF16), pltpu.VMEM(narrow, BF16),
            dma((2, 9)), dma((2, 9)), dma((5,)),
        ],
        compiler_params=pltpu.CompilerParams(
            collective_id=0, has_side_effects=True, vmem_limit_bytes=60 * 2**20
        ),
        name="gather_forward",
    )(tokens_in, out_grad, norm_gain.reshape(1, d), gate_weight, up_weight, down_weight)
    normed, whole_grad, hidden, ggp, gup = [a.reshape(flat + a.shape[2:]) for a in gathered]
    local_down = jnp.dot(hidden.T, whole_grad, preferred_element_type=F32).astype(BF16)
    local_gate = jnp.dot(normed.T, ggp, preferred_element_type=F32).astype(BF16)
    local_up = jnp.dot(normed.T, gup, preferred_element_type=F32).astype(BF16)
    tall, long = (d, ff), (ff, d)
    block4 = (4, rows, d)
    grad_normed, sum_down, sum_gate, sum_up = pl.pallas_call(
        lambda *refs: exit_kernel(reps, *refs),
        out_shape=[
            jax.ShapeDtypeStruct((rows, d), F32),
            jax.ShapeDtypeStruct(long, BF16),
            jax.ShapeDtypeStruct(tall, BF16),
            jax.ShapeDtypeStruct(tall, BF16),
        ],
        in_specs=[vmem] * 7,
        out_specs=[vmem] * 4,
        scratch_shapes=[
            pltpu.VMEM(long, BF16), pltpu.VMEM(tall, BF16), pltpu.VMEM(tall, BF16),
            pltpu.VMEM(block4, BF16), pltpu.VMEM(block4, BF16), pltpu.VMEM(block4, BF16), pltpu.VMEM(block4, BF16),
            dma((3, CHUNKS)), dma((3, CHUNKS)), dma((3, CHUNKS)), dma((3, CHUNKS)),
            dma((4,)), dma((4,)), dma((4,)), dma((4,)),
        ],
        compiler_params=pltpu.CompilerParams(
            collective_id=1, has_side_effects=True, vmem_limit_bytes=60 * 2**20
        ),
        name="reduce_exit",
    )(ggp, gup, gate_weight, up_weight, local_down, local_gate, local_up)
    grad_gate = sum_gate.astype(F32) * factor
    grad_up = sum_up.astype(F32) * factor
    grad_down = sum_down.astype(F32) * (0.5 * factor)
    floats = tokens_in.astype(F32)
    inverse = lax.rsqrt(jnp.mean(floats * floats, axis=-1, keepdims=True) + norm_eps)
    unit = floats * inverse
    grad_gain = lax.psum(jnp.sum(grad_normed * unit, axis=0), ("rep", "fs", "tp"))
    scaled = grad_normed * norm_gain
    grad_in = (
        out_grad.astype(F32)
        + inverse * scaled
        - unit * inverse * jnp.mean(scaled * unit, axis=-1, keepdims=True)
    )
    return (grad_in.astype(BF16), grad_gain, grad_gate, grad_up, grad_down)


def solution(mesh):
    spread = ("fs", "tp")
    in_specs = (
        P(("rep", "fs", "tp"), None), P(), P(None, spread), P(None, spread), P(spread, None),
        P(("rep", "fs", "tp"), None),
    )
    out_specs = (
        P(("rep", "fs", "tp"), None), P(), P(None, spread), P(None, spread), P(spread, None),
    )
    return jax.shard_map(shards, mesh=mesh, in_specs=in_specs, out_specs=out_specs, check_vma=False)
```

profile of v0, /device:TPU:0, one launch (start us, length us, event | category | flops | bytes accessed | tf_op | source)
XLA Modules:
  0.0 296.5 jit_solution(9877854991352534400)
XLA Ops:
  0.6 85.5 %gather_forward.1 = (bf16[8,256,2048]{2,1,0:T(8,128)(2,1)}, bf16[8,256,2048]{2,1,0:T(8,128)(2,1)}, bf16[8,256,384]{2,1,0:T(8,128)(2,1)}, bf16[8,256,384]{2,1,0:T(8,128)(2,1)}, bf16[8,256,384]{2,1,0:T(8,128)(2,1)}) custom-call(bf16[256,2048]{1,0:T(8,128)(2,1)} %x_ref.1, bf16[256,2048]{1,0:T(8,128)(2,1)} %g_ref.1, f32[1,2048]{1,0:T(1,128)} %bitcast.17, ...), custom_call_target="tpu_custom_call" | custom-call | tf_op jit(solution)/shard_map/gather_forward/pallas_call | solution.py:316
  86.2 0.0 copy-start.5
  86.2 0.0 copy-start.8
  86.2 8.6 %bitcast_convert_fusion.2.refs_4_ = bf16[384,2048]{1,0:T(8,128)(2,1)} fusion(bf16[8,256,384]{2,1,0:T(8,128)(2,1)} %get-tuple-element.16, bf16[8,256,2048]{2,1,0:T(8,128)(2,1)} %get-tuple-element.17), kind=kOutput, calls=%fused_computation.2 | convolution fusion | flops 3222011904 | bytes 11534336 | tf_op jit(solution)/shard_map/dot_general | solution.py:332
  94.8 0.0 copy-done.5
  94.8 0.0 copy-done.8
  94.8 0.0 copy-start.6
  94.8 5.6 %bitcast_convert_fusion.1.refs_5_ = bf16[2048,384]{1,0:T(8,128)(2,1)} fusion(bf16[8,256,2048]{2,1,0:T(8,128)(2,1)S(1)} %copy-done.8, bf16[8,256,384]{2,1,0:T(8,128)(2,1)S(1)} %copy-done.5), kind=kOutput, calls=%fused_computation.1 | convolution fusion | flops 3222011904 | bytes 11534336 | tf_op jit(solution)/shard_map/dot_general | solution.py:333
  100.5 0.0 copy-done.6
  100.5 5.6 %bitcast_convert_fusion.refs_6_ = bf16[2048,384]{1,0:T(8,128)(2,1)} fusion(bf16[8,256,2048]{2,1,0:T(8,128)(2,1)S(1)} %copy-done.8, bf16[8,256,384]{2,1,0:T(8,128)(2,1)S(1)} %copy-done.6), kind=kOutput, calls=%fused_computation | convolution fusion | flops 3222011904 | bytes 11534336 | tf_op jit(solution)/shard_map/dot_general | solution.py:334
  106.1 0.0 copy-start
  106.1 0.0 copy-start.7
  106.1 140.2 %reduce_exit.1 = (f32[256,2048]{1,0:T(8,128)}, bf16[384,2048]{1,0:T(8,128)(2,1)}, bf16[2048,384]{1,0:T(8,128)(2,1)}, bf16[2048,384]{1,0:T(8,128)(2,1)}) custom-call(bf16[2048,384]{1,0:T(8,128)(2,1)} %bitcast.15, bf16[2048,384]{1,0:T(8,128)(2,1)} %bitcast.16, bf16[2048,384]{1,0:T(8,128)(2,1)} %refs_2_.1, bf16[2048,384]{1,0:T(8,128)(2,1)} %refs_3_.1, ...), custom_call_target="tpu_custom_call" | custom-call | tf_op jit(solution)/shard_map/reduce_exit/pallas_call | solution.py:337
  246.3 0.0 copy-done
  246.3 0.0 copy-start.1
  246.3 0.0 copy-start.2
  246.3 0.3 fusion.8
  246.6 0.0 copy-done.7
  246.6 2.4 fusion.7
  249.1 0.0 copy-done.1
  249.1 0.0 copy-done.2
  249.1 0.0 copy-start.3
  249.1 1.8 fusion.5
  250.9 38.8 %psum.7 = f32[2048]{0:T(1024)} all-reduce(f32[2048]{0:T(1024)S(1)} %get-tuple-element.23), channel_id=1, replica_groups=mesh['rep'=4,'fs'=4,'tp'=2] {'rep','fs','tp'}, use_global_device_ids=true, to_apply=%region_3.0 | all-reduce | flops 2048 | bytes 16384 | tf_op jit(solution)/shard_map/psum | solution.py:364
  289.6 0.0 copy-done.3
  289.6 0.0 copy-start.4
  289.6 4.8 %convert_multiply_fusion.1 = (f32[2048,384]{1,0:T(8,128)}, f32[2048,384]{1,0:T(8,128)}) fusion(bf16[2048,384]{1,0:T(8,128)(2,1)} %get-tuple-element.21, bf16[2048,384]{1,0:T(8,128)(2,1)S(1)} %copy-done.3), kind=kLoop, calls=%fused_computation.4 | loop fusion | flops 3145728 | bytes 9437184 | tf_op jit(solution)/shard_map/mul | solution.py:359
  294.4 0.0 copy-done.4
  294.4 2.1 convert_multiply_fusion
  (2 shorter events, 0.0 us)
Async XLA Ops:
  86.2 8.6 %copy-start.5 = (bf16[8,256,384]{2,1,0:T(8,128)(2,1)S(1)}, bf16[8,256,384]{2,1,0:T(8,128)(2,1)}, u32[]{:S(2)}) copy-start(bf16[8,256,384]{2,1,0:T(8,128)(2,1)} %get-tuple-element.14) | copy-start | bytes 4718596
  86.2 8.6 %copy-start.8 = (bf16[8,256,2048]{2,1,0:T(8,128)(2,1)S(1)}, bf16[8,256,2048]{2,1,0:T(8,128)(2,1)}, u32[]{:S(2)}) copy-start(bf16[8,256,2048]{2,1,0:T(8,128)(2,1)} %get-tuple-element.18) | copy-start | bytes 25165828
  94.8 5.6 %copy-start.6 = (bf16[8,256,384]{2,1,0:T(8,128)(2,1)S(1)}, bf16[8,256,384]{2,1,0:T(8,128)(2,1)}, u32[]{:S(2)}) copy-start(bf16[8,256,384]{2,1,0:T(8,128)(2,1)} %get-tuple-element.15) | copy-start | bytes 4718596
  106.1 140.2 %copy-start = (bf16[256,2048]{1,0:T(8,128)(2,1)S(1)}, bf16[256,2048]{1,0:T(8,128)(2,1)}, u32[]{:S(2)}) copy-start(bf16[256,2048]{1,0:T(8,128)(2,1)} %x_ref.1) | copy-start | bytes 3145732
  106.1 140.5 %copy-start.7 = (f32[2048]{0:T(1024)S(1)}, f32[2048]{0:T(1024)}, u32[]{:S(2)}) copy-start(f32[2048]{0:T(1024)} %param.7) | copy-start | bytes 24580
  246.3 2.7 copy-start.1
  246.3 2.7 copy-start.2
  249.1 40.6 %copy-start.3 = (bf16[2048,384]{1,0:T(8,128)(2,1)S(1)}, bf16[2048,384]{1,0:T(8,128)(2,1)}, u32[]{:S(2)}) copy-start(bf16[2048,384]{1,0:T(8,128)(2,1)} %get-tuple-element.20) | copy-start | bytes 4718596
  289.6 4.8 %copy-start.4 = (bf16[384,2048]{1,0:T(8,128)(2,1)S(1)}, bf16[384,2048]{1,0:T(8,128)(2,1)}, u32[]{:S(2)}) copy-start(bf16[384,2048]{1,0:T(8,128)(2,1)} %get-tuple-element.22) | copy-start | bytes 4718596
where the time goes:
time: 297 us; the launch traced here: 296 us
  Pallas kernels  226 us (76%)
  blocking collectives  38.8 us (13%)
  matrix products  19.9 us (7%)
  other arithmetic  11.3 us (4%)
    pallas_call x1, Pallas kernels, shards(): pl.pallas_call(lambda *refs: exit_kernel(reps, *refs), out_shape=[jax.Sha...  140 us
    pallas_call x1, Pallas kernels, shards(): pl.pallas_call(gather_kernel, out_shape=[jax.ShapeDtypeStruct(s, BF16) fo...  85.5 us
    psum x1, blocking collectives, shards(): lax.psum(jnp.sum(grad_normed * unit, axis=0), ('rep', 'fs', 'tp'))  38.8 us
    dot_general x1, matrix products, shards(): jnp.dot(hidden.T, whole_grad, preferred_element_type=F32).astype(BF16)  8.62 us

commit v1 on v0

v1 whole, which is shorter than its diff:
```python
import jax
import jax.numpy as jnp
from jax import lax
from jax.experimental import pallas as pl
from jax.experimental.pallas import tpu as pltpu
from jax.sharding import PartitionSpec as P

norm_eps = 1e-06
MESH = pl.DeviceIdType.MESH
F32, BF16 = jnp.float32, jnp.bfloat16
NT = (((1,), (1,)), ((), ()))
PARTS = 8
AHEAD = 2
SUB = 2
LAG_IN = 1
LAG_FIN = 3
LAG_OUT = 5
EXIT_TICK = 2 * PARTS + 2
FINISH = 30


def flip(f, j):
    return (f % 2 + j % 2) % 2 + 2 * ((f // 2 + j // 2) % 2)


def remote(src, dst, send, recv, dev):
    return pltpu.make_async_remote_copy(
        src_ref=src, dst_ref=dst, send_sem=send, recv_sem=recv, device_id=dev, device_id_type=MESH
    )


def fused_kernel(
    reps, factor,
    x_hbm, g_hbm, gain_ref, gw_hbm, uw_hbm, dw_hbm,
    gi_out, gg_out, down_out, gate_out, up_out,
    nall, gall, wcat, dwc, act, gh, tcat, gcat, own, inc, fin,
    tbuf, pin, rsin, xbuf, stage_d, stage_g, gv, gr, grep,
    ssem, rsem, lsem, up_send, in_recv, down_send, fin_recv,
    p_send, p_recv, s_send, s_recv, v_send, v_recv, w_send, w_recv, osem,
):
    f, t, r = lax.axis_index("fs"), lax.axis_index("tp"), lax.axis_index("rep")
    other = 1 - t
    parts, rk, d = xbuf.shape
    rows = parts * rk
    ff = dwc.shape[1]
    cw = d // parts
    ranks = gcat.shape[1]
    toks = ranks * rk
    chunks = 3 * parts
    sub = ff // SUB

    middle = reps // 2
    sign = 1 - 2 * (r // middle)
    up, down = {"rep": r + sign}, {"rep": (r - sign + reps) % reps}
    right = r // middle
    depth = (1 - right) * (middle - 1 - r) + right * (r - middle)
    center, outer = depth == 0, depth == middle - 1
    inner, has_down = depth > 0, depth < middle - 1
    to_a, to_b, to_p = {"fs": flip(f, 1)}, {"fs": flip(f, 2)}, {"tp": other}

    barrier = pltpu.get_barrier_semaphore()
    for dev in (to_a, to_b, {"fs": flip(f, 3)}, to_p):
        pl.semaphore_signal(barrier, inc=1, device_id=dev, device_id_type=MESH)
    for i in range(1, reps):
        pl.semaphore_signal(barrier, inc=1, device_id={"rep": (r + i) % reps}, device_id_type=MESH)

    def pos(j, core):
        return flip(f, j) * 2 + core

    me = pos(0, t)

    def loads():
        out = [pltpu.make_async_copy(x_hbm, xbuf, lsem.at[0])]
        out.append(pltpu.make_async_copy(gw_hbm, wcat.at[:, pl.ds(0, ff)], lsem.at[1]))
        out.append(pltpu.make_async_copy(uw_hbm, wcat.at[:, pl.ds(ff, ff)], lsem.at[2]))
        for c in range(parts):
            cols = pl.ds(c * cw, cw)
            out.append(pltpu.make_async_copy(g_hbm.at[:, :, cols], gall.at[c, :, me], lsem.at[3 + c]))
        for c in range(parts):
            cols = pl.ds(c * cw, cw)
            out.append(pltpu.make_async_copy(dw_hbm.at[:, cols], dwc.at[c], lsem.at[3 + parts + c]))
        return out

    local = loads()
    for c in local:
        c.start()

    def slot(ph, k, p, part=0):
        if ph == 0:
            ref = nall.at[k, p]
            size = rk // 2
        else:
            ref = gall.at[k, :, p]
            size = parts // 2
        if part == 0:
            return ref
        return ref.at[pl.ds((part - 1) * size, size)]

    def copy(ph, k, kind, incoming=False):
        sems = (ssem.at[kind, ph * parts + k], rsem.at[kind, ph * parts + k])
        core = other if incoming else t
        if kind == 0:
            ref, dev = slot(ph, k, pos(1, t) if incoming else me), to_a
        elif kind == 1:
            ref, dev = slot(ph, k, pos(2, t) if incoming else me), to_b
        elif kind == 2:
            ref, dev = slot(ph, k, pos(0, core)), to_p
        elif kind == 3:
            ref, dev = slot(ph, k, pos(3, t) if incoming else pos(1, t), 2), to_b
        elif kind == 4:
            ref, dev = slot(ph, k, pos(3, t) if incoming else pos(2, t), 1), to_a
        elif kind == 5:
            ref, dev = slot(ph, k, pos(1, core)), to_p
        elif kind == 6:
            ref, dev = slot(ph, k, pos(2, core)), to_p
        else:
            ref, dev = slot(ph, k, pos(3, core), kind - 6), to_p
        return remote(ref, ref, *sems, dev)

    def normalise(k):
        floats = xbuf[k].astype(F32)
        inverse = lax.rsqrt(jnp.mean(floats * floats, axis=-1, keepdims=True) + norm_eps)
        nall[k, me] = (floats * inverse * gain_ref[...]).astype(BF16)

    def issue(ph, k):
        if ph == 0:
            normalise(k)
        for kind in (0, 1, 2):
            copy(ph, k, kind).start()

    local[0].wait()
    pl.semaphore_wait(barrier, 3 + reps)
    for k in range(AHEAD):
        issue(0, k)
    for c in local[3:3 + parts]:
        c.wait()

    def forward(k):
        block = nall[k].reshape(toks, d)
        pre = jnp.dot(block, wcat[...], preferred_element_type=F32)
        gate_pre, up_pre = pre[:, :ff], pre[:, ff:]
        sigma = jax.nn.sigmoid(gate_pre)
        active = gate_pre * sigma
        act[k, :, pl.ds(0, ff)] = up_pre * sigma * (1.0 + gate_pre * (1.0 - sigma))
        act[k, :, pl.ds(ff, ff)] = active
        cols = pl.ds(pl.multiple_of(k * toks, toks), toks)
        tcat[pl.ds(0, ff), cols] = (active * up_pre).T.astype(BF16)

    def grad_chunk(c):
        whole = gall[c].reshape(parts * toks, cw)
        own[c] = jnp.dot(tcat[pl.ds(0, ff), :], whole, preferred_element_type=F32).astype(BF16)

        def one(k, carry):
            block = gall[c, k].reshape(toks, cw)
            part = lax.dot_general(block, dwc[c], NT, preferred_element_type=F32)

            @pl.when(c == 0)
            def _():
                gh[k] = part

            @pl.when(c > 0)
            def _():
                gh[k] = gh[k] + part

            return carry

        lax.fori_loop(0, parts, one, 0)

    def elementwise(k, carry):
        half = 0.5 * gh[k]
        ggp = half * act[k, :, pl.ds(0, ff)]
        gup = half * act[k, :, pl.ds(ff, ff)]
        cols = pl.ds(pl.multiple_of(k * toks, toks), toks)
        gcat[k, :, :, pl.ds(0, ff)] = ggp.astype(BF16).reshape(ranks, rk, ff)
        gcat[k, :, :, pl.ds(ff, ff)] = gup.astype(BF16).reshape(ranks, rk, ff)
        tcat[pl.ds(0, ff), cols] = ggp.T.astype(BF16)
        tcat[pl.ds(ff, ff), cols] = gup.T.astype(BF16)
        return carry

    def weight_chunk(s):
        a, c = s // parts - 1, s % parts
        left = tcat[pl.ds(pl.multiple_of(a * ff, ff), ff), :]
        cols = pl.ds(pl.multiple_of(c * cw, cw), cw)
        whole = nall[:, :, :, cols].reshape(parts * toks, cw)
        own[s] = jnp.dot(left, whole, preferred_element_type=F32).astype(BF16)

    def piece(ref, s, h):
        return ref.at[s, pl.ds(h * sub, sub)]

    def up_copy(s, h, src, dst, recv):
        return remote(piece(src, s, h), piece(dst, s, h), up_send.at[s, h], recv.at[s, h], up)

    def down_copy(s, h):
        return remote(piece(fin, s, h), piece(fin, s, h), down_send.at[s, h], fin_recv.at[s, h], down)

    def down_store(s):
        cols = pl.ds(pl.multiple_of(s * cw, cw), cw)
        return pltpu.make_async_copy(stage_d.at[s % 2], down_out.at[:, cols], osem.at[s % 2])

    def gate_store(s, out):
        here = pl.ds(pl.multiple_of((s % parts) * cw, cw), cw)
        return pltpu.make_async_copy(stage_g.at[s % 2], out.at[here], osem.at[2 + s % 2])

    def emit(s):
        @pl.when(s < parts)
        def _():
            @pl.when(s >= 2)
            def _():
                down_store(s - 2).wait()

            stage_d[s % 2] = fin[s].astype(F32) * (0.5 * factor)
            down_store(s).start()

        @pl.when(s >= parts)
        def _():
            @pl.when(s >= parts + 2)
            def _():
                gate_store(s - 2, gate_out).wait()

            stage_g[s % 2] = (fin[s].astype(F32) * factor).T

            @pl.when(s < 2 * parts)
            def _():
                gate_store(s, gate_out).start()

            @pl.when(s >= 2 * parts)
            def _():
                gate_store(s, up_out).start()

    def reduce_step(z):
        @pl.when(outer & (z >= 0) & (z < chunks))
        def _():
            for h in range(SUB):
                @pl.when(center)
                def _():
                    up_copy(z, h, own, fin, fin_recv).start()

                @pl.when(inner)
                def _():
                    up_copy(z, h, own, inc, in_recv).start()

        s_in = z - LAG_IN

        @pl.when(has_down & (s_in >= 0) & (s_in < chunks))
        def _():
            for h in range(SUB):
                up_copy(s_in, h, inc, inc, in_recv).wait_recv()
                here = piece(inc, s_in, h)
                here[...] = (piece(own, s_in, h)[...].astype(F32) + here[...].astype(F32)).astype(BF16)

                @pl.when(center)
                def _():
                    up_copy(s_in, h, inc, fin, fin_recv).start()

                @pl.when(inner)
                def _():
                    up_copy(s_in, h, inc, inc, in_recv).start()

        s_fin = z - jnp.where(center, LAG_FIN, LAG_OUT)

        @pl.when((s_fin >= 0) & (s_fin < chunks))
        def _():
            for h in range(SUB):
                down_copy(s_fin, h).wait_recv()
                here = piece(fin, s_fin, h)

                @pl.when(center & has_down)
                def _():
                    here[...] = (piece(inc, s_fin, h)[...].astype(F32) + here[...].astype(F32)).astype(BF16)

                @pl.when(center & outer)
                def _():
                    here[...] = (piece(own, s_fin, h)[...].astype(F32) + here[...].astype(F32)).astype(BF16)

                @pl.when(has_down)
                def _():
                    down_copy(s_fin, h).start()

            emit(s_fin)

    def pair_copy(j):
        return remote(tbuf.at[(3 - j) % 2], pin.at[j], p_send.at[j], p_recv.at[j], to_p)

    def peer_copy(j):
        return remote(pin.at[j], rsin.at[j - 1], s_send.at[j], s_recv.at[j], {"fs": flip(f, j)})

    def term(owner, c):
        cols = pl.ds(pl.multiple_of(c * cw, cw), cw)
        block = gcat[:, owner].reshape(rows, 2 * ff)
        return lax.dot_general(block, wcat[cols, :], NT, preferred_element_type=F32).astype(BF16), cols

    def exit_step(i):
        @pl.when((i >= 0) & (i < 4))
        def _():
            j = 3 - i

            @pl.when(i >= 2)
            def _():
                pair_copy(j + 2).wait_send()

            def one(c, carry):
                value, cols = term(flip(f, j) * 2 + other, c)
                tbuf[i % 2, :, cols] = value
                return carry

            lax.fori_loop(0, parts, one, 0)
            pair_copy(j).start()

        @pl.when((i >= 1) & (i < 5))
        def _():
            j = 4 - i
            pair_copy(j).wait_recv()

            def one(c, carry):
                value, cols = term(flip(f, j) * 2 + t, c)
                total = value.astype(F32) + pin[j, :, cols].astype(F32)
                gh[c, :, pl.ds(0, cw)] = total
                pin[j, :, cols] = total.astype(BF16)
                return carry

            lax.fori_loop(0, parts, one, 0)

            @pl.when(j > 0)
            def _():
                peer_copy(j).start()

    def vec_copy(n):
        dev = (to_p, to_a, to_b)[n]
        return remote(gv.at[n], gr.at[n], v_send.at[n], v_recv.at[n], dev)

    def rep_copy(i, incoming=False):
        at = (r - i + reps) % reps if incoming else r
        return remote(grep.at[at], grep.at[at], w_send.at[i], w_recv.at[i], {"rep": (r + i) % reps})

    def finish():
        for j in (3, 2, 1):
            peer_copy(j).wait_recv()
        gv[0] = jnp.zeros_like(gv[0])

        def one(k, carry):
            here = pl.ds(pl.multiple_of(k * rk, rk), rk)
            grads = jnp.concatenate([gh[c, here, pl.ds(0, cw)] for c in range(parts)], axis=1)
            for j in (2, 1, 0):
                grads = grads + rsin[j, here, :].astype(F32)
            floats = xbuf[k].astype(F32)
            inverse = lax.rsqrt(jnp.mean(floats * floats, axis=-1, keepdims=True) + norm_eps)
            unit = floats * inverse
            gv[0] = gv[0] + jnp.sum(grads * unit, axis=0, keepdims=True)
            scaled = grads * gain_ref[...]
            shift = inverse * jnp.mean(scaled * unit, axis=-1, keepdims=True)
            cot = jnp.concatenate([gall[c, k, me] for c in range(parts)], axis=1).astype(F32)
            xbuf[k] = (cot + inverse * scaled - unit * shift).astype(BF16)
            return carry

        lax.fori_loop(0, parts, one, 0)
        pltpu.make_async_copy(xbuf, gi_out, lsem.at[0]).start()
        vec_copy(0).start()

    def tick(q, carry):
        for ph in (0, 1):
            k = q - ph * parts

            @pl.when((k >= 0) & (k < parts))
            def _():
                copy(ph, k, 0, True).wait_recv()
                copy(ph, k, 3).start()
                copy(ph, k, 5).start()
                copy(ph, k, 1, True).wait_recv()
                copy(ph, k, 4).start()
                copy(ph, k, 6).start()

        for ph in (0, 1):
            k = q + AHEAD - ph * parts

            @pl.when((k >= 0) & (k < parts))
            def _():
                issue(ph, k)

        @pl.when(q == 2)
        def _():
            for c in local[1:3]:
                c.wait()

        @pl.when(q == parts + 2)
        def _():
            for c in local[3 + parts:]:
                c.wait()

        for ph in (0, 1):
            k = q - 2 - ph * parts

            @pl.when((k >= 0) & (k < parts))
            def _():
                for kind in (2, 5, 6, 7, 8):
                    copy(ph, k, kind, True).wait_recv()
                if ph == 0:
                    forward(k)
                else:
                    grad_chunk(k)

        z = q - parts - 2

        @pl.when((z >= parts) & (z < chunks))
        def _():
            weight_chunk(z)

        reduce_step(z)

        for ph in (0, 1):
            k = q - 1 - ph * parts

            @pl.when((k >= 0) & (k < parts))
            def _():
                copy(ph, k, 3, True).wait_recv()
                copy(ph, k, 8).start()
                copy(ph, k, 4, True).wait_recv()
                copy(ph, k, 7).start()

        @pl.when(q == EXIT_TICK - 1)
        def _():
            lax.fori_loop(0, parts, elementwise, 0)

        exit_step(q - EXIT_TICK)

        @pl.when(q == FINISH)
        def _():
            finish()

        for n in (0, 1, 2):
            @pl.when(q == FINISH + 1 + n)
            def _():
                vec_copy(n).wait_recv()
                gv[n + 1] = gv[n] + gr[n]
                if n < 2:
                    vec_copy(n + 1).start()
                else:
                    grep[r] = gv[3]
                    for i in range(1, reps):
                        rep_copy(i).start()

        return carry

    ticks = parts + 2 + chunks + LAG_OUT
    lax.fori_loop(0, ticks, tick, 0)

    for i in range(1, reps):
        rep_copy(i, True).wait_recv()
    total = grep[0]
    for i in range(1, reps):
        total = total + grep[i]
    for n in range(3):
        vec_copy(n).wait_send()
    gv[0] = total
    last = pltpu.make_async_copy(gv.at[0], gg_out, lsem.at[1])
    last.start()

    def drain(k, carry):
        for ph in (0, 1):
            for kind in range(9):
                copy(ph, k, kind).wait_send()
        return carry

    lax.fori_loop(0, parts, drain, 0)

    def drain_reduce(s, carry):
        for h in range(SUB):
            up_copy(s, h, own, inc, in_recv).wait_send()

            @pl.when(has_down)
            def _():
                down_copy(s, h).wait_send()

        return carry

    lax.fori_loop(0, chunks, drain_reduce, 0)
    for j in (1, 0):
        pair_copy(j).wait_send()
    for j in (3, 2, 1):
        peer_copy(j).wait_send()
    for i in range(1, reps):
        rep_copy(i).wait_send()
    for s in (parts - 2, parts - 1):
        down_store(s).wait()
    for s in (chunks - 2, chunks - 1):
        gate_store(s, up_out).wait()
    pltpu.make_async_copy(xbuf, gi_out, lsem.at[0]).wait()
    last.wait()


def shards(tokens_in, norm_gain, gate_weight, up_weight, down_weight, out_grad):
    rows, d = tokens_in.shape
    ff = gate_weight.shape[1]
    reps = lax.axis_size("rep")
    ranks = lax.axis_size("fs") * lax.axis_size("tp")
    factor = float(rows * reps * ranks) ** (-0.5)
    rk, cw = rows // PARTS, d // PARTS
    vmem, anywhere = pl.BlockSpec(memory_space=pltpu.VMEM), pl.BlockSpec(memory_space=pl.ANY)
    dma = pltpu.SemaphoreType.DMA
    chunks = 3 * PARTS
    shape = lambda *s: jax.ShapeDtypeStruct(s, F32)
    narrow = lambda *s: pltpu.VMEM(s, BF16)
    wide = lambda *s: pltpu.VMEM(s, F32)
    grad_in, grad_gain, grad_down, grad_gate, grad_up = pl.pallas_call(
        lambda *refs: fused_kernel(reps, factor, *refs),
        out_shape=[
            jax.ShapeDtypeStruct((PARTS, rk, d), BF16), shape(1, d), shape(ff, d), shape(d, ff), shape(d, ff),
        ],
        in_specs=[anywhere, anywhere, vmem, anywhere, anywhere, anywhere],
        out_specs=[anywhere] * 5,
        scratch_shapes=[
            narrow(PARTS, ranks, rk, d), narrow(PARTS, PARTS, ranks, rk, cw),
            narrow(d, 2 * ff), narrow(PARTS, ff, cw),
            wide(PARTS, ranks * rk, 2 * ff), wide(PARTS, ranks * rk, ff),
            narrow(2 * ff, PARTS * ranks * rk), narrow(PARTS, ranks, rk, 2 * ff),
            narrow(chunks, ff, cw), narrow(chunks, ff, cw), narrow(chunks, ff, cw),
            narrow(2, rows, d), narrow(4, rows, d), narrow(3, rows, d), narrow(PARTS, rk, d),
            wide(2, ff, cw), wide(2, cw, ff), wide(4, 1, d), wide(3, 1, d), wide(reps, 1, d),
            dma((9, 2 * PARTS)), dma((9, 2 * PARTS)), dma((3 + 2 * PARTS,)),
            dma((chunks, SUB)), dma((chunks, SUB)), dma((chunks, SUB)), dma((chunks, SUB)),
            dma((4,)), dma((4,)), dma((4,)), dma((4,)), dma((3,)), dma((3,)), dma((reps,)), dma((reps,)), dma((4,)),
        ],
        compiler_params=pltpu.CompilerParams(
            collective_id=0, has_side_effects=True, vmem_limit_bytes=63 * 2**20
        ),
        name="fused_backward",
    )(
        tokens_in.reshape(PARTS, rk, d), out_grad.reshape(PARTS, rk, d), norm_gain.reshape(1, d),
        gate_weight, up_weight, down_weight,
    )
    return (grad_in.reshape(rows, d), grad_gain.reshape(d), grad_gate, grad_up, grad_down)


def solution(mesh):
    spread = ("fs", "tp")
    in_specs = (
        P(("rep", "fs", "tp"), None), P(), P(None, spread), P(None, spread), P(spread, None),
        P(("rep", "fs", "tp"), None),
    )
    out_specs = (
        P(("rep", "fs", "tp"), None), P(), P(None, spread), P(None, spread), P(spread, None),
    )
    return jax.shard_map(shards, mesh=mesh, in_specs=in_specs, out_specs=out_specs, check_vma=False)
```

time: 297 us -> 198 us (0.67)
  Pallas kernels: 226 us -> 184 us
  blocking collectives: 38.8 us -> 0 us
  matrix products: 19.9 us -> 0 us
  local copies, waits for them, and re-layouts: 0.04 us -> 12.2 us
  other arithmetic: 11.3 us -> 0 us
    pallas_call x2 -> x1, Pallas kernels: 226 us -> 184 us  [shards(): pl.pallas_call(lambda *refs: fused_kernel(reps, factor, *refs), out_shape...]
    psum x1 -> x0, blocking collectives: 38.8 us -> none  [shards(): lax.psum(jnp.sum(grad_normed * unit, axis=0), ('rep', 'fs', 'tp'))]
    dot_general x3 -> x0, matrix products: 19.9 us -> none  [the longest x1 8.62 us: shards(): jnp.dot(hidden.T, whole_grad, preferred_element_type=F32).astype(BF16)]
    unnamed x18 -> x9, local copies, waits for them, and re-layouts: 0.04 us -> 12.2 us
    mul x2 -> x0, other arithmetic: 6.84 us -> none  [the longest x1 4.78 us: shards(): grad_up = sum_up.astype(F32) * factor]
where the time goes in v1:
time: 198 us; the launch traced here: 197 us
  Pallas kernels  184 us (93%)
  local copies, waits for them, and re-layouts  12.2 us (6%)
    pallas_call x1, Pallas kernels, shards(): pl.pallas_call(lambda *refs: fused_kernel(reps, factor, *refs), out_shape...  184 us
    unnamed x9, local copies, waits for them, and re-layouts  12.2 us

profile of v1, /device:TPU:0, one launch (start us, length us, event | category | flops | bytes accessed | tf_op | source)
XLA Modules:
  0.0 197.3 jit_solution(3301080946295462422)
XLA Ops:
  0.6 184.5 %fused_backward.1 = (bf16[8,32,2048]{2,1,0:T(8,128)(2,1)}, f32[1,2048]{1,0:T(1,128)}, f32[384,2048]{1,0:T(8,128)}, f32[2048,384]{1,0:T(8,128)}, f32[2048,384]{1,0:T(8,128)}) custom-call(bf16[8,32,2048]{2,1,0:T(8,128)(2,1)} %bitcast.6, bf16[8,32,2048]{2,1,0:T(8,128)(2,1)} %bitcast.7, f32[1,2048]{1,0:T(1,128)} %bitcast.8, bf16[2048,384]{1,0:T(8,128)(2,1)} %refs_3_.1, ...), custom_call_target="tpu_custom_call" | custom-call | tf_op jit(solution)/shard_map/fused_backward/pallas_call | solution.py:503
  185.1 2.3 %copy.16 = bf16[256,2048]{1,0:T(8,128)(2,1)} copy(bf16[256,2048]{1,0:T(8,128)(2,1)} %bitcast.5) | data formatting | bytes 2097152
  187.4 1.3 copy.17
  188.7 0.0 copy-start.1
  188.7 3.9 %copy.18 = f32[2048,384]{1,0:T(8,128)} copy(f32[2048,384]{1,0:T(8,128)} %get-tuple-element.22) | data formatting | bytes 6291456
  192.6 0.0 copy-done.1
  192.6 0.0 copy-start
  192.6 1.7 copy.19
  194.3 1.4 copy-done
  195.7 1.7 copy.20
Async XLA Ops:
  188.7 3.9 %copy-start.1 = (f32[2048,384]{1,0:T(8,128)S(1)}, f32[2048,384]{1,0:T(8,128)}, u32[]{:S(2)}) copy-start(f32[2048,384]{1,0:T(8,128)} %get-tuple-element.23) | copy-start | bytes 9437188
  192.6 3.0 %copy-start = (f32[384,2048]{1,0:T(8,128)S(1)}, f32[384,2048]{1,0:T(8,128)}, u32[]{:S(2)}) copy-start(f32[384,2048]{1,0:T(8,128)} %get-tuple-element.24) | copy-start | bytes 9437188

commit v2 on v1

--- a/solution.py
+++ b/solution.py
@@ -11,12 +11,15 @@
 NT = (((1,), (1,)), ((), ()))
 PARTS = 8
 AHEAD = 2
+PIECES = 4
 SUB = 2
 LAG_IN = 1
 LAG_FIN = 3
-LAG_OUT = 5
+LAG_OUT = 6
 EXIT_TICK = 2 * PARTS + 2
-FINISH = 30
+UNROLL = 4
+LAG_SEND = 4
+FINISH = 31
 
 
 def flip(f, j):
@@ -30,11 +33,11 @@
 
 
 def fused_kernel(
-    reps, factor,
+    reps,
     x_hbm, g_hbm, gain_ref, gw_hbm, uw_hbm, dw_hbm,
     gi_out, gg_out, down_out, gate_out, up_out,
-    nall, gall, wcat, dwc, act, gh, tcat, gcat, own, inc, fin,
-    tbuf, pin, rsin, xbuf, stage_d, stage_g, gv, gr, grep,
+    nall, gall, wcat, dwt, act, gh, tcat, gcat, own, inc, fin,
+    tbuf, pin, rsin, xbuf, stage_g, gv, gr, grep,
     ssem, rsem, lsem, up_send, in_recv, down_send, fin_recv,
     p_send, p_recv, s_send, s_recv, v_send, v_recv, w_send, w_recv, osem,
 ):
@@ -42,12 +45,13 @@
     other = 1 - t
     parts, rk, d = xbuf.shape
     rows = parts * rk
-    ff = dwc.shape[1]
+    ff = dwt.shape[2]
     cw = d // parts
     ranks = gcat.shape[1]
     toks = ranks * rk
     chunks = 3 * parts
     sub = ff // SUB
+    turn = 2 * ff // toks
 
     middle = reps // 2
     sign = 1 - 2 * (r // middle)
@@ -78,7 +82,7 @@
             out.append(pltpu.make_async_copy(g_hbm.at[:, :, cols], gall.at[c, :, me], lsem.at[3 + c]))
         for c in range(parts):
             cols = pl.ds(c * cw, cw)
-            out.append(pltpu.make_async_copy(dw_hbm.at[:, cols], dwc.at[c], lsem.at[3 + parts + c]))
+            out.append(pltpu.make_async_copy(dw_hbm.at[:, cols], own.at[2 * parts + c], lsem.at[3 + parts + c]))
         return out
 
     local = loads()
@@ -123,12 +127,12 @@
         nall[k, me] = (floats * inverse * gain_ref[...]).astype(BF16)
 
     def issue(ph, k):
-        if ph == 0:
-            normalise(k)
         for kind in (0, 1, 2):
             copy(ph, k, kind).start()
 
     local[0].wait()
+    for k in range(AHEAD):
+        normalise(k)
     pl.semaphore_wait(barrier, 3 + reps)
     for k in range(AHEAD):
         issue(0, k)
@@ -150,21 +154,15 @@
         whole = gall[c].reshape(parts * toks, cw)
         own[c] = jnp.dot(tcat[pl.ds(0, ff), :], whole, preferred_element_type=F32).astype(BF16)
 
-        def one(k, carry):
-            block = gall[c, k].reshape(toks, cw)
-            part = lax.dot_general(block, dwc[c], NT, preferred_element_type=F32)
-
-            @pl.when(c == 0)
-            def _():
-                gh[k] = part
-
-            @pl.when(c > 0)
-            def _():
-                gh[k] = gh[k] + part
-
+    def accumulate(c):
+        def one(i, carry):
+            for n in range(UNROLL):
+                k = i * UNROLL + n
+                block = gall[c, k].reshape(toks, cw)
+                gh[k] = gh[k] + jnp.dot(block, dwt[c], preferred_element_type=F32)
             return carry
 
-        lax.fori_loop(0, parts, one, 0)
+        lax.fori_loop(0, parts // UNROLL, one, 0)
 
     def elementwise(k, carry):
         half = 0.5 * gh[k]
@@ -177,12 +175,12 @@
         tcat[pl.ds(ff, ff), cols] = gup.T.astype(BF16)
         return carry
 
-    def weight_chunk(s):
-        a, c = s // parts - 1, s % parts
-        left = tcat[pl.ds(pl.multiple_of(a * ff, ff), ff), :]
+    def weight_pair(c):
         cols = pl.ds(pl.multiple_of(c * cw, cw), cw)
         whole = nall[:, :, :, cols].reshape(parts * toks, cw)
-        own[s] = jnp.dot(left, whole, preferred_element_type=F32).astype(BF16)
+        both = jnp.dot(tcat[...], whole, preferred_element_type=F32).astype(BF16)
+        own[parts + 2 * c] = both[:ff]
+        own[parts + 2 * c + 1] = both[ff:]
 
     def piece(ref, s, h):
         return ref.at[s, pl.ds(h * sub, sub)]
@@ -195,10 +193,10 @@
 
     def down_store(s):
         cols = pl.ds(pl.multiple_of(s * cw, cw), cw)
-        return pltpu.make_async_copy(stage_d.at[s % 2], down_out.at[:, cols], osem.at[s % 2])
+        return pltpu.make_async_copy(fin.at[s], down_out.at[:, cols], osem.at[s % 2])
 
     def gate_store(s, out):
-        here = pl.ds(pl.multiple_of((s % parts) * cw, cw), cw)
+        here = pl.ds(pl.multiple_of(((s - parts) // 2) * cw, cw), cw)
         return pltpu.make_async_copy(stage_g.at[s % 2], out.at[here], osem.at[2 + s % 2])
 
     def emit(s):
@@ -208,7 +206,6 @@
             def _():
                 down_store(s - 2).wait()
 
-            stage_d[s % 2] = fin[s].astype(F32) * (0.5 * factor)
             down_store(s).start()
 
         @pl.when(s >= parts)
@@ -217,28 +214,37 @@
             def _():
                 gate_store(s - 2, gate_out).wait()
 
-            stage_g[s % 2] = (fin[s].astype(F32) * factor).T
-
-            @pl.when(s < 2 * parts)
+            stage_g[s % 2] = fin[s].T
+
+            @pl.when(s % 2 == 0)
             def _():
                 gate_store(s, gate_out).start()
 
-            @pl.when(s >= 2 * parts)
+            @pl.when(s % 2 == 1)
             def _():
                 gate_store(s, up_out).start()
 
-    def reduce_step(z):
-        @pl.when(outer & (z >= 0) & (z < chunks))
+    def send_own(s):
+        @pl.when(outer)
         def _():
             for h in range(SUB):
                 @pl.when(center)
                 def _():
-                    up_copy(z, h, own, fin, fin_recv).start()
+                    up_copy(s, h, own, fin, fin_recv).start()
 
                 @pl.when(inner)
                 def _():
-                    up_copy(z, h, own, inc, in_recv).start()
-
+                    up_copy(s, h, own, inc, in_recv).start()
+
+    def settle(s):
+        for h in range(SUB):
+            up_copy(s, h, own, inc, in_recv).wait_send()
+
+            @pl.when(has_down)
+            def _():
+                down_copy(s, h).wait_send()
+
+    def reduce_step(z):
         s_in = z - LAG_IN
 
         @pl.when(has_down & (s_in >= 0) & (s_in < chunks))
@@ -278,6 +284,12 @@
 
             emit(s_fin)
 
+        s_old = s_fin - LAG_SEND
+
+        @pl.when((s_old >= 0) & (s_old < chunks))
+        def _():
+            settle(s_old)
+
     def pair_copy(j):
         return remote(tbuf.at[(3 - j) % 2], pin.at[j], p_send.at[j], p_recv.at[j], to_p)
 
@@ -287,38 +299,46 @@
     def term(owner, c):
         cols = pl.ds(pl.multiple_of(c * cw, cw), cw)
         block = gcat[:, owner].reshape(rows, 2 * ff)
-        return lax.dot_general(block, wcat[cols, :], NT, preferred_element_type=F32).astype(BF16), cols
+        right = gall[c, pl.ds(0, turn)].reshape(2 * ff, cw)
+        return jnp.dot(block, right, preferred_element_type=F32).astype(BF16), cols
+
+    def turn_weights(c, carry):
+        here = pl.ds(pl.multiple_of(c * cw, cw), cw)
+        gall[c, pl.ds(0, turn)] = wcat[here, :].T.reshape(turn, ranks, rk, cw)
+        return carry
 
     def exit_step(i):
-        @pl.when((i >= 0) & (i < 4))
-        def _():
-            j = 3 - i
-
-            @pl.when(i >= 2)
+        j = 3 - i // 2
+
+        @pl.when((i >= 0) & (i < 8) & (i % 2 == 0))
+        def _():
+            @pl.when(j < 2)
             def _():
                 pair_copy(j + 2).wait_send()
 
-            def one(c, carry):
-                value, cols = term(flip(f, j) * 2 + other, c)
-                tbuf[i % 2, :, cols] = value
+            def one(i, carry):
+                for n in range(UNROLL):
+                    value, cols = term(flip(f, j) * 2 + other, i * UNROLL + n)
+                    tbuf[(3 - j) % 2, :, cols] = value
                 return carry
 
-            lax.fori_loop(0, parts, one, 0)
+            lax.fori_loop(0, parts // UNROLL, one, 0)
             pair_copy(j).start()
 
-        @pl.when((i >= 1) & (i < 5))
-        def _():
-            j = 4 - i
+        @pl.when((i >= 0) & (i < 8) & (i % 2 == 1))
+        def _():
             pair_copy(j).wait_recv()
 
-            def one(c, carry):
-                value, cols = term(flip(f, j) * 2 + t, c)
-                total = value.astype(F32) + pin[j, :, cols].astype(F32)
-                gh[c, :, pl.ds(0, cw)] = total
-                pin[j, :, cols] = total.astype(BF16)
+            def one(i, carry):
+                for n in range(UNROLL):
+                    c = i * UNROLL + n
+                    value, cols = term(flip(f, j) * 2 + t, c)
+                    total = value.astype(F32) + pin[j, :, cols].astype(F32)
+                    gh[c, :, pl.ds(0, cw)] = total
+                    pin[j, :, cols] = total.astype(BF16)
                 return carry
 
-            lax.fori_loop(0, parts, one, 0)
+            lax.fori_loop(0, parts // UNROLL, one, 0)
 
             @pl.when(j > 0)
             def _():
@@ -332,7 +352,12 @@
         at = (r - i + reps) % reps if incoming else r
         return remote(grep.at[at], grep.at[at], w_send.at[i], w_recv.at[i], {"rep": (r + i) % reps})
 
+    def reload(k):
+        return pltpu.make_async_copy(g_hbm.at[k], tbuf.at[0, pl.ds(k * rk, rk)], lsem.at[3 + k])
+
     def finish():
+        for k in range(parts):
+            reload(k).wait()
         for j in (3, 2, 1):
             peer_copy(j).wait_recv()
         gv[0] = jnp.zeros_like(gv[0])
@@ -348,13 +373,21 @@
             gv[0] = gv[0] + jnp.sum(grads * unit, axis=0, keepdims=True)
             scaled = grads * gain_ref[...]
             shift = inverse * jnp.mean(scaled * unit, axis=-1, keepdims=True)
-            cot = jnp.concatenate([gall[c, k, me] for c in range(parts)], axis=1).astype(F32)
+            cot = tbuf[0, here, :].astype(F32)
             xbuf[k] = (cot + inverse * scaled - unit * shift).astype(BF16)
             return carry
 
         lax.fori_loop(0, parts, one, 0)
         pltpu.make_async_copy(xbuf, gi_out, lsem.at[0]).start()
         vec_copy(0).start()
+
+    def drain(ph):
+        def one(k, carry):
+            for kind in range(9):
+                copy(ph, k, kind).wait_send()
+            return carry
+
+        return one
 
     def tick(q, carry):
         for ph in (0, 1):
@@ -374,23 +407,40 @@
 
             @pl.when((k >= 0) & (k < parts))
             def _():
+                if ph == 0:
+                    normalise(k)
                 issue(ph, k)
 
-        @pl.when(q == 2)
-        def _():
-            for c in local[1:3]:
+        @pl.when(q == 1)
+        def _():
+            for c in local[1:3] + local[3 + parts:]:
                 c.wait()
 
-        @pl.when(q == parts + 2)
-        def _():
-            for c in local[3 + parts:]:
-                c.wait()
+            def clear(k, carry):
+                gh[k] = jnp.zeros_like(gh[k])
+                return carry
+
+            lax.fori_loop(0, parts, clear, 0)
+
+        @pl.when((q >= 2) & (q < parts + 2))
+        def _():
+            dwt[q - 2] = own[2 * parts + q - 2].T
+
+        late = q - 2 - parts
+
+        @pl.when((late >= 0) & (late < parts - 1))
+        def _():
+            accumulate(late)
 
         for ph in (0, 1):
-            k = q - 2 - ph * parts
+            k = q - 1 - ph * parts
 
             @pl.when((k >= 0) & (k < parts))
             def _():
+                copy(ph, k, 3, True).wait_recv()
+                copy(ph, k, 8).start()
+                copy(ph, k, 4, True).wait_recv()
+                copy(ph, k, 7).start()
                 for kind in (2, 5, 6, 7, 8):
                     copy(ph, k, kind, True).wait_recv()
                 if ph == 0:
@@ -398,27 +448,37 @@
                 else:
                     grad_chunk(k)
 
-        z = q - parts - 2
-
-        @pl.when((z >= parts) & (z < chunks))
-        def _():
-            weight_chunk(z)
+        z = q - parts - 1
+
+        @pl.when((z >= 0) & (z < parts))
+        def _():
+            send_own(z)
+
+        @pl.when((z >= parts) & (z < 2 * parts))
+        def _():
+            weight_pair(z - parts)
+            send_own(2 * z - parts)
+            send_own(2 * z - parts + 1)
 
         reduce_step(z)
 
-        for ph in (0, 1):
-            k = q - 1 - ph * parts
-
-            @pl.when((k >= 0) & (k < parts))
-            def _():
-                copy(ph, k, 3, True).wait_recv()
-                copy(ph, k, 8).start()
-                copy(ph, k, 4, True).wait_recv()
-                copy(ph, k, 7).start()
+        @pl.when(q == 2 * parts)
+        def _():
+            accumulate(parts - 1)
+            lax.fori_loop(0, parts, elementwise, 0)
 
         @pl.when(q == EXIT_TICK - 1)
         def _():
-            lax.fori_loop(0, parts, elementwise, 0)
+            for ph in (0, 1):
+                lax.fori_loop(0, parts, drain(ph), 0)
+            lax.fori_loop(0, parts, turn_weights, 0)
+
+        @pl.when(q == EXIT_TICK + 8)
+        def _():
+            for j in (1, 0):
+                pair_copy(j).wait_send()
+            for k in range(parts):
+                reload(k).start()
 
         exit_step(q - EXIT_TICK)
 
@@ -440,7 +500,7 @@
 
         return carry
 
-    ticks = parts + 2 + chunks + LAG_OUT
+    ticks = parts + 1 + chunks + LAG_OUT
     lax.fori_loop(0, ticks, tick, 0)
 
     for i in range(1, reps):
@@ -454,27 +514,16 @@
     last = pltpu.make_async_copy(gv.at[0], gg_out, lsem.at[1])
     last.start()
 
-    def drain(k, carry):
-        for ph in (0, 1):
-            for kind in range(9):
-                copy(ph, k, kind).wait_send()
+    last_fin = ticks - 1 - parts - 1 - jnp.where(center, LAG_FIN, LAG_OUT)
+
+    def settle_rest(s, carry):
+        @pl.when(s > last_fin - LAG_SEND)
+        def _():
+            settle(s)
+
         return carry
 
-    lax.fori_loop(0, parts, drain, 0)
-
-    def drain_reduce(s, carry):
-        for h in range(SUB):
-            up_copy(s, h, own, inc, in_recv).wait_send()
-
-            @pl.when(has_down)
-            def _():
-                down_copy(s, h).wait_send()
-
-        return carry
-
-    lax.fori_loop(0, chunks, drain_reduce, 0)
-    for j in (1, 0):
-        pair_copy(j).wait_send()
+    lax.fori_loop(chunks - LAG_SEND, chunks, settle_rest, 0)
     for j in (3, 2, 1):
         peer_copy(j).wait_send()
     for i in range(1, reps):
@@ -485,6 +534,43 @@
         gate_store(s, up_out).wait()
     pltpu.make_async_copy(xbuf, gi_out, lsem.at[0]).wait()
     last.wait()
+
+
+def widen_kernel(factor, *refs):
+    arrays, rest = refs[:3], refs[3:5]
+    outs, rest_outs = refs[5:8], refs[8:10]
+    taken, given, held = refs[10:13], refs[13:16], refs[16:18]
+    isem, osem, rsem, wsem = refs[18:]
+
+    def rows(a, i):
+        size = arrays[a].shape[0] // PIECES
+        return pl.ds(i * size, size)
+
+    def take(a, i):
+        return pltpu.make_async_copy(arrays[a].at[rows(a, i)], taken[a].at[rows(a, i)], isem.at[a, i])
+
+    def give(a, i):
+        return pltpu.make_async_copy(given[a].at[rows(a, i)], outs[a].at[rows(a, i)], osem.at[a, i])
+
+    order = [(a, i) for a in range(3) for i in range(PIECES)]
+    for a, i in order:
+        take(a, i).start()
+    carried = [pltpu.make_async_copy(rest[n], held[n], rsem.at[n]) for n in range(2)]
+    passed = [pltpu.make_async_copy(held[n], rest_outs[n], wsem.at[n]) for n in range(2)]
+    for c in carried:
+        c.start()
+    for a, i in order:
+        take(a, i).wait()
+        scale = 0.5 * factor if a == 0 else factor
+        given[a][rows(a, i), :] = taken[a][rows(a, i), :].astype(F32) * scale
+        give(a, i).start()
+    for n in range(2):
+        carried[n].wait()
+        passed[n].start()
+    for a, i in order:
+        give(a, i).wait()
+    for c in passed:
+        c.wait()
 
 
 def shards(tokens_in, norm_gain, gate_weight, up_weight, down_weight, out_grad):
@@ -498,23 +584,24 @@
     dma = pltpu.SemaphoreType.DMA
     chunks = 3 * PARTS
     shape = lambda *s: jax.ShapeDtypeStruct(s, F32)
+    half = lambda *s: jax.ShapeDtypeStruct(s, BF16)
     narrow = lambda *s: pltpu.VMEM(s, BF16)
     wide = lambda *s: pltpu.VMEM(s, F32)
     grad_in, grad_gain, grad_down, grad_gate, grad_up = pl.pallas_call(
-        lambda *refs: fused_kernel(reps, factor, *refs),
+        lambda *refs: fused_kernel(reps, *refs),
         out_shape=[
-            jax.ShapeDtypeStruct((PARTS, rk, d), BF16), shape(1, d), shape(ff, d), shape(d, ff), shape(d, ff),
+            half(PARTS, rk, d), shape(1, d), half(ff, d), half(d, ff), half(d, ff),
         ],
         in_specs=[anywhere, anywhere, vmem, anywhere, anywhere, anywhere],
         out_specs=[anywhere] * 5,
         scratch_shapes=[
             narrow(PARTS, ranks, rk, d), narrow(PARTS, PARTS, ranks, rk, cw),
-            narrow(d, 2 * ff), narrow(PARTS, ff, cw),
+            narrow(d, 2 * ff), narrow(PARTS, cw, ff),
             wide(PARTS, ranks * rk, 2 * ff), wide(PARTS, ranks * rk, ff),
             narrow(2 * ff, PARTS * ranks * rk), narrow(PARTS, ranks, rk, 2 * ff),
             narrow(chunks, ff, cw), narrow(chunks, ff, cw), narrow(chunks, ff, cw),
             narrow(2, rows, d), narrow(4, rows, d), narrow(3, rows, d), narrow(PARTS, rk, d),
-            wide(2, ff, cw), wide(2, cw, ff), wide(4, 1, d), wide(3, 1, d), wide(reps, 1, d),
+            narrow(2, cw, ff), wide(4, 1, d), wide(3, 1, d), wide(reps, 1, d),
             dma((9, 2 * PARTS)), dma((9, 2 * PARTS)), dma((3 + 2 * PARTS,)),
             dma((chunks, SUB)), dma((chunks, SUB)), dma((chunks, SUB)), dma((chunks, SUB)),
             dma((4,)), dma((4,)), dma((4,)), dma((4,)), dma((3,)), dma((3,)), dma((reps,)), dma((reps,)), dma((4,)),
@@ -527,7 +614,20 @@
         tokens_in.reshape(PARTS, rk, d), out_grad.reshape(PARTS, rk, d), norm_gain.reshape(1, d),
         gate_weight, up_weight, down_weight,
     )
-    return (grad_in.reshape(rows, d), grad_gain.reshape(d), grad_gate, grad_up, grad_down)
+    arrays = (grad_down, grad_gate, grad_up)
+    outs = [shape(*a.shape) for a in arrays]
+    grad_down, grad_gate, grad_up, grad_in, grad_gain = pl.pallas_call(
+        lambda *refs: widen_kernel(factor, *refs),
+        out_shape=outs + [half(rows, d), shape(1, d)],
+        in_specs=[anywhere] * 5,
+        out_specs=[anywhere] * 5,
+        scratch_shapes=[narrow(*a.shape) for a in arrays] + [wide(*a.shape) for a in arrays] + [
+            narrow(rows, d), wide(1, d), dma((3, PIECES)), dma((3, PIECES)), dma((2,)), dma((2,)),
+        ],
+        compiler_params=pltpu.CompilerParams(vmem_limit_bytes=63 * 2**20),
+        name="widen",
+    )(grad_down, grad_gate, grad_up, grad_in.reshape(rows, d), grad_gain)
+    return (grad_in, grad_gain.reshape(d), grad_gate, grad_up, grad_down)
 
 
 def solution(mesh):

time: 198 us -> 181 us (0.914)
  local copies, waits for them, and re-layouts: 12.2 us -> 0 us
  Pallas kernels: 184 us -> 180 us
    unnamed x9 -> x0, local copies, waits for them, and re-layouts: 12.2 us -> none
    pallas_call x1 -> x2, Pallas kernels: 184 us -> 180 us  [the longest x1 175 us: shards(): pl.pallas_call(lambda *refs: fused_kernel(reps, *refs), out_shape=[half(P...]
where the time goes in v2:
time: 181 us
  Pallas kernels  180 us (99%)
    pallas_call x1, Pallas kernels, shards(): pl.pallas_call(lambda *refs: fused_kernel(reps, *refs), out_shape=[half(P...  175 us
    pallas_call x1, Pallas kernels, shards(): pl.pallas_call(lambda *refs: widen_kernel(factor, *refs), out_shape=outs...  5.76 us

profile of v2, /device:TPU:0, one launch (start us, length us, event | category | flops | bytes accessed | tf_op | source)
XLA Modules:
  0.0 180.9 jit_solution(8555996741166144851)
XLA Ops:
  0.6 174.5 %fused_backward.1 = (bf16[8,32,2048]{2,1,0:T(8,128)(2,1)}, f32[1,2048]{1,0:T(1,128)}, bf16[384,2048]{1,0:T(8,128)(2,1)}, bf16[2048,384]{1,0:T(8,128)(2,1)}, bf16[2048,384]{1,0:T(8,128)(2,1)}) custom-call(bf16[8,32,2048]{2,1,0:T(8,128)(2,1)} %bitcast.5, bf16[8,32,2048]{2,1,0:T(8,128)(2,1)} %bitcast.6, f32[1,2048]{1,0:T(1,128)} %bitcast.8, ...), custom_call_target="tpu_custom_call" | custom-call | tf_op jit(solution)/shard_map/fused_backward/pallas_call | solution.py:590
  175.2 5.8 %widen.1 = (f32[384,2048]{1,0:T(8,128)}, f32[2048,384]{1,0:T(8,128)}, f32[2048,384]{1,0:T(8,128)}, bf16[256,2048]{1,0:T(8,128)(2,1)}, f32[1,2048]{1,0:T(1,128)}) custom-call(bf16[384,2048]{1,0:T(8,128)(2,1)} %get-tuple-element.15.refs_0_, bf16[2048,384]{1,0:T(8,128)(2,1)} %get-tuple-element.16.refs_1_, bf16[2048,384]{1,0:T(8,128)(2,1)} %get-tuple-element.17.refs_2_, ...), custom_call_target="tpu_custom_call" | custom-call | tf_op jit(solution)/shard_map/widen/pallas_call | solution.py:619

commit v3 on v2

--- a/solution.py
+++ b/solution.py
@@ -14,11 +14,10 @@
 PIECES = 4
 SUB = 2
 LAG_IN = 1
-LAG_FIN = 3
+LAG_FIN = 2
 LAG_OUT = 6
 EXIT_TICK = 2 * PARTS + 2
 UNROLL = 4
-LAG_SEND = 4
 FINISH = 31
 
 
@@ -51,6 +50,7 @@
     toks = ranks * rk
     chunks = 3 * parts
     sub = ff // SUB
+    ticks = parts + 1 + chunks + LAG_OUT
     turn = 2 * ff // toks
 
     middle = reps // 2
@@ -101,7 +101,7 @@
         return ref.at[pl.ds((part - 1) * size, size)]
 
     def copy(ph, k, kind, incoming=False):
-        sems = (ssem.at[kind, ph * parts + k], rsem.at[kind, ph * parts + k])
+        sems = (ssem.at[kind, ph], rsem.at[kind, k])
         core = other if incoming else t
         if kind == 0:
             ref, dev = slot(ph, k, pos(1, t) if incoming else me), to_a
@@ -186,10 +186,10 @@
         return ref.at[s, pl.ds(h * sub, sub)]
 
     def up_copy(s, h, src, dst, recv):
-        return remote(piece(src, s, h), piece(dst, s, h), up_send.at[s, h], recv.at[s, h], up)
+        return remote(piece(src, s, h), piece(dst, s, h), up_send.at[0], recv.at[s, h], up)
 
     def down_copy(s, h):
-        return remote(piece(fin, s, h), piece(fin, s, h), down_send.at[s, h], fin_recv.at[s, h], down)
+        return remote(piece(fin, s, h), piece(fin, s, h), down_send.at[0], fin_recv.at[s, h], down)
 
     def down_store(s):
         cols = pl.ds(pl.multiple_of(s * cw, cw), cw)
@@ -236,59 +236,63 @@
                 def _():
                     up_copy(s, h, own, inc, in_recv).start()
 
-    def settle(s):
+    def take_in(s, h):
+        @pl.when(has_down & (s >= 0) & (s < chunks))
+        def _():
+            up_copy(s, h, inc, inc, in_recv).wait_recv()
+            here = piece(inc, s, h)
+            here[...] = (piece(own, s, h)[...].astype(F32) + here[...].astype(F32)).astype(BF16)
+
+            @pl.when(center)
+            def _():
+                up_copy(s, h, inc, fin, fin_recv).start()
+
+            @pl.when(inner)
+            def _():
+                up_copy(s, h, inc, inc, in_recv).start()
+
+    def take_fin(s, h):
+        down_copy(s, h).wait_recv()
+        here = piece(fin, s, h)
+
+        @pl.when(center & has_down)
+        def _():
+            here[...] = (piece(inc, s, h)[...].astype(F32) + here[...].astype(F32)).astype(BF16)
+
+        @pl.when(center & outer)
+        def _():
+            here[...] = (piece(own, s, h)[...].astype(F32) + here[...].astype(F32)).astype(BF16)
+
+        @pl.when(has_down)
+        def _():
+            down_copy(s, h).start()
+
+    def reduce_step(z):
         for h in range(SUB):
-            up_copy(s, h, own, inc, in_recv).wait_send()
-
-            @pl.when(has_down)
-            def _():
-                down_copy(s, h).wait_send()
-
-    def reduce_step(z):
-        s_in = z - LAG_IN
-
-        @pl.when(has_down & (s_in >= 0) & (s_in < chunks))
+            take_in(z - LAG_IN, h)
+
+        s_mid = z - LAG_FIN
+
+        @pl.when(center & has_down & (s_mid >= 0) & (s_mid < chunks))
+        def _():
+            for h in range(SUB - 1):
+                take_fin(s_mid, h)
+
+        s_fin = z - LAG_OUT
+
+        @pl.when((s_fin >= 0) & (s_fin < chunks) & (outer | inner))
         def _():
             for h in range(SUB):
-                up_copy(s_in, h, inc, inc, in_recv).wait_recv()
-                here = piece(inc, s_in, h)
-                here[...] = (piece(own, s_in, h)[...].astype(F32) + here[...].astype(F32)).astype(BF16)
-
-                @pl.when(center)
-                def _():
-                    up_copy(s_in, h, inc, fin, fin_recv).start()
-
-                @pl.when(inner)
-                def _():
-                    up_copy(s_in, h, inc, inc, in_recv).start()
-
-        s_fin = z - jnp.where(center, LAG_FIN, LAG_OUT)
-
-        @pl.when((s_fin >= 0) & (s_fin < chunks))
-        def _():
-            for h in range(SUB):
-                down_copy(s_fin, h).wait_recv()
-                here = piece(fin, s_fin, h)
-
-                @pl.when(center & has_down)
-                def _():
-                    here[...] = (piece(inc, s_fin, h)[...].astype(F32) + here[...].astype(F32)).astype(BF16)
-
-                @pl.when(center & outer)
-                def _():
-                    here[...] = (piece(own, s_fin, h)[...].astype(F32) + here[...].astype(F32)).astype(BF16)
-
-                @pl.when(has_down)
-                def _():
-                    down_copy(s_fin, h).start()
-
+                take_fin(s_fin, h)
             emit(s_fin)
 
-        s_old = s_fin - LAG_SEND
-
-        @pl.when((s_old >= 0) & (s_old < chunks))
-        def _():
-            settle(s_old)
+    def reduce_rest(z):
+        s_mid = z - LAG_FIN - 1
+
+        @pl.when(center & has_down & (s_mid >= 0) & (s_mid < chunks))
+        def _():
+            take_fin(s_mid, SUB - 1)
+            emit(s_mid)
 
     def pair_copy(j):
         return remote(tbuf.at[(3 - j) % 2], pin.at[j], p_send.at[j], p_recv.at[j], to_p)
@@ -382,12 +386,30 @@
         vec_copy(0).start()
 
     def drain(ph):
-        def one(k, carry):
-            for kind in range(9):
-                copy(ph, k, kind).wait_send()
-            return carry
-
-        return one
+        places = (me, me, me, pos(1, t), pos(2, t), pos(1, t), pos(2, t), pos(3, t), pos(3, t))
+        for kind, p in enumerate(places):
+            part = {3: 2, 4: 1, 7: 1, 8: 2}.get(kind, 0)
+            if ph == 0:
+                size = rk // 2 if part else rk
+                ref = nall.at[:, p, pl.ds(max(part - 1, 0) * size, size)]
+            else:
+                size = parts // 2 if part else parts
+                ref = gall.at[:, pl.ds(max(part - 1, 0) * size, size), p]
+            remote(ref, ref, ssem.at[kind, ph], rsem.at[kind, 0], to_p).wait_send()
+
+    def gain_store():
+        return pltpu.make_async_copy(gv.at[0], gg_out, lsem.at[1])
+
+    def gain_total():
+        for i in range(1, reps):
+            rep_copy(i, True).wait_recv()
+        total = grep[0]
+        for i in range(1, reps):
+            total = total + grep[i]
+        for n in range(3):
+            vec_copy(n).wait_send()
+        gv[0] = total
+        gain_store().start()
 
     def tick(q, carry):
         for ph in (0, 1):
@@ -431,6 +453,9 @@
         @pl.when((late >= 0) & (late < parts - 1))
         def _():
             accumulate(late)
+
+        z = q - parts - 1
+        reduce_rest(z)
 
         for ph in (0, 1):
             k = q - 1 - ph * parts
@@ -448,8 +473,6 @@
                 else:
                     grad_chunk(k)
 
-        z = q - parts - 1
-
         @pl.when((z >= 0) & (z < parts))
         def _():
             send_own(z)
@@ -469,8 +492,8 @@
 
         @pl.when(q == EXIT_TICK - 1)
         def _():
-            for ph in (0, 1):
-                lax.fori_loop(0, parts, drain(ph), 0)
+            drain(0)
+            drain(1)
             lax.fori_loop(0, parts, turn_weights, 0)
 
         @pl.when(q == EXIT_TICK + 8)
@@ -498,32 +521,20 @@
                     for i in range(1, reps):
                         rep_copy(i).start()
 
+        @pl.when(q == ticks - 1)
+        def _():
+            gain_total()
+
         return carry
 
-    ticks = parts + 1 + chunks + LAG_OUT
     lax.fori_loop(0, ticks, tick, 0)
 
-    for i in range(1, reps):
-        rep_copy(i, True).wait_recv()
-    total = grep[0]
-    for i in range(1, reps):
-        total = total + grep[i]
-    for n in range(3):
-        vec_copy(n).wait_send()
-    gv[0] = total
-    last = pltpu.make_async_copy(gv.at[0], gg_out, lsem.at[1])
-    last.start()
-
-    last_fin = ticks - 1 - parts - 1 - jnp.where(center, LAG_FIN, LAG_OUT)
-
-    def settle_rest(s, carry):
-        @pl.when(s > last_fin - LAG_SEND)
-        def _():
-            settle(s)
-
-        return carry
-
-    lax.fori_loop(chunks - LAG_SEND, chunks, settle_rest, 0)
+    remote(own, inc, up_send.at[0], in_recv.at[0, 0], up).wait_send()
+
+    @pl.when(has_down)
+    def _():
+        remote(fin, fin, down_send.at[0], fin_recv.at[0, 0], down).wait_send()
+
     for j in (3, 2, 1):
         peer_copy(j).wait_send()
     for i in range(1, reps):
@@ -533,7 +544,7 @@
     for s in (chunks - 2, chunks - 1):
         gate_store(s, up_out).wait()
     pltpu.make_async_copy(xbuf, gi_out, lsem.at[0]).wait()
-    last.wait()
+    gain_store().wait()
 
 
 def widen_kernel(factor, *refs):
@@ -602,8 +613,8 @@
             narrow(chunks, ff, cw), narrow(chunks, ff, cw), narrow(chunks, ff, cw),
             narrow(2, rows, d), narrow(4, rows, d), narrow(3, rows, d), narrow(PARTS, rk, d),
             narrow(2, cw, ff), wide(4, 1, d), wide(3, 1, d), wide(reps, 1, d),
-            dma((9, 2 * PARTS)), dma((9, 2 * PARTS)), dma((3 + 2 * PARTS,)),
-            dma((chunks, SUB)), dma((chunks, SUB)), dma((chunks, SUB)), dma((chunks, SUB)),
+            dma((9, 2)), dma((9, PARTS)), dma((3 + 2 * PARTS,)),
+            dma((1,)), dma((chunks, SUB)), dma((1,)), dma((chunks, SUB)),
             dma((4,)), dma((4,)), dma((4,)), dma((4,)), dma((3,)), dma((3,)), dma((reps,)), dma((reps,)), dma((4,)),
         ],
         compiler_params=pltpu.CompilerParams(

time: 181 us -> 175 us (0.967)
  Pallas kernels: 180 us -> 174 us
    pallas_call x1, Pallas kernels: 175 us -> 168 us  [shards(): pl.pallas_call(lambda *refs: fused_kernel(reps, *refs), out_shape=[half(P...]
where the time goes in v3:
time: 175 us; the launch traced here: 174 us
  Pallas kernels  174 us (99%)
    pallas_call x1, Pallas kernels, shards(): pl.pallas_call(lambda *refs: fused_kernel(reps, *refs), out_shape=[half(P...  168 us
    pallas_call x1, Pallas kernels, shards(): pl.pallas_call(lambda *refs: widen_kernel(factor, *refs), out_shape=outs...  5.76 us

profile of v3, /device:TPU:0, one launch (start us, length us, event | category | flops | bytes accessed | tf_op | source)
XLA Modules:
  0.0 174.5 jit_solution(14696383020573938108)
XLA Ops:
  0.6 168.1 %fused_backward.1 = (bf16[8,32,2048]{2,1,0:T(8,128)(2,1)}, f32[1,2048]{1,0:T(1,128)}, bf16[384,2048]{1,0:T(8,128)(2,1)}, bf16[2048,384]{1,0:T(8,128)(2,1)}, bf16[2048,384]{1,0:T(8,128)(2,1)}) custom-call(bf16[8,32,2048]{2,1,0:T(8,128)(2,1)} %bitcast.5, bf16[8,32,2048]{2,1,0:T(8,128)(2,1)} %bitcast.6, f32[1,2048]{1,0:T(1,128)} %bitcast.8, ...), custom_call_target="tpu_custom_call" | custom-call | tf_op jit(solution)/shard_map/fused_backward/pallas_call | solution.py:601
  168.7 5.8 %widen.1 = (f32[384,2048]{1,0:T(8,128)}, f32[2048,384]{1,0:T(8,128)}, f32[2048,384]{1,0:T(8,128)}, bf16[256,2048]{1,0:T(8,128)(2,1)}, f32[1,2048]{1,0:T(1,128)}) custom-call(bf16[384,2048]{1,0:T(8,128)(2,1)} %get-tuple-element.15.refs_0_, bf16[2048,384]{1,0:T(8,128)(2,1)} %get-tuple-element.16.refs_1_, bf16[2048,384]{1,0:T(8,128)(2,1)} %get-tuple-element.17.refs_2_, ...), custom_call_target="tpu_custom_call" | custom-call | tf_op jit(solution)/shard_map/widen/pallas_call | solution.py:630

commit v4 on v3

--- a/solution.py
+++ b/solution.py
@@ -11,13 +11,13 @@
 NT = (((1,), (1,)), ((), ()))
 PARTS = 8
 AHEAD = 2
-PIECES = 4
+PIECES = 2
 SUB = 2
 LAG_IN = 1
 LAG_FIN = 2
 LAG_OUT = 6
 EXIT_TICK = 2 * PARTS + 2
-UNROLL = 4
+UNROLL = 8
 FINISH = 31
 
 

time: 175 us -> 174 us (level)
  no operation moved by 1% of the time
where the time goes in v4:
time: 174 us
  Pallas kernels  173 us (99%)
    pallas_call x1, Pallas kernels, shards(): pl.pallas_call(lambda *refs: fused_kernel(reps, *refs), out_shape=[half(P...  168 us
    pallas_call x1, Pallas kernels, shards(): pl.pallas_call(lambda *refs: widen_kernel(factor, *refs), out_shape=outs...  5.48 us

profile of v4, /device:TPU:0, one launch (start us, length us, event | category | flops | bytes accessed | tf_op | source)
XLA Modules:
  0.0 173.8 jit_solution(14916057750151249742)
XLA Ops:
  0.6 167.7 %fused_backward.1 = (bf16[8,32,2048]{2,1,0:T(8,128)(2,1)}, f32[1,2048]{1,0:T(1,128)}, bf16[384,2048]{1,0:T(8,128)(2,1)}, bf16[2048,384]{1,0:T(8,128)(2,1)}, bf16[2048,384]{1,0:T(8,128)(2,1)}) custom-call(bf16[8,32,2048]{2,1,0:T(8,128)(2,1)} %bitcast.5, bf16[8,32,2048]{2,1,0:T(8,128)(2,1)} %bitcast.6, f32[1,2048]{1,0:T(1,128)} %bitcast.8, ...), custom_call_target="tpu_custom_call" | custom-call | tf_op jit(solution)/shard_map/fused_backward/pallas_call | solution.py:601
  168.4 5.5 %widen.1 = (f32[384,2048]{1,0:T(8,128)}, f32[2048,384]{1,0:T(8,128)}, f32[2048,384]{1,0:T(8,128)}, bf16[256,2048]{1,0:T(8,128)(2,1)}, f32[1,2048]{1,0:T(1,128)}) custom-call(bf16[384,2048]{1,0:T(8,128)(2,1)} %get-tuple-element.15.refs_0_, bf16[2048,384]{1,0:T(8,128)(2,1)} %get-tuple-element.16.refs_1_, bf16[2048,384]{1,0:T(8,128)(2,1)} %get-tuple-element.17.refs_2_, ...), custom_call_target="tpu_custom_call" | custom-call | tf_op jit(solution)/shard_map/widen/pallas_call | solution.py:630

commit v5 on v4

--- a/solution.py
+++ b/solution.py
@@ -82,7 +82,7 @@
             out.append(pltpu.make_async_copy(g_hbm.at[:, :, cols], gall.at[c, :, me], lsem.at[3 + c]))
         for c in range(parts):
             cols = pl.ds(c * cw, cw)
-            out.append(pltpu.make_async_copy(dw_hbm.at[:, cols], own.at[2 * parts + c], lsem.at[3 + parts + c]))
+            out.append(pltpu.make_async_copy(dw_hbm.at[:, cols], own.at[2 * parts + c], lsem.at[3 + parts]))
         return out
 
     local = loads()
@@ -435,8 +435,10 @@
 
         @pl.when(q == 1)
         def _():
-            for c in local[1:3] + local[3 + parts:]:
+            for c in local[1:3]:
                 c.wait()
+            raw = own.at[pl.ds(2 * parts, parts)]
+            pltpu.make_async_copy(raw, raw, lsem.at[3 + parts]).wait()
 
             def clear(k, carry):
                 gh[k] = jnp.zeros_like(gh[k])
@@ -613,7 +615,7 @@
             narrow(chunks, ff, cw), narrow(chunks, ff, cw), narrow(chunks, ff, cw),
             narrow(2, rows, d), narrow(4, rows, d), narrow(3, rows, d), narrow(PARTS, rk, d),
             narrow(2, cw, ff), wide(4, 1, d), wide(3, 1, d), wide(reps, 1, d),
-            dma((9, 2)), dma((9, PARTS)), dma((3 + 2 * PARTS,)),
+            dma((9, 2)), dma((9, PARTS)), dma((4 + PARTS,)),
             dma((1,)), dma((chunks, SUB)), dma((1,)), dma((chunks, SUB)),
             dma((4,)), dma((4,)), dma((4,)), dma((4,)), dma((3,)), dma((3,)), dma((reps,)), dma((reps,)), dma((4,)),
         ],

time: 174 us -> 174 us (level)
  no operation moved by 1% of the time
where the time goes in v5:
time: 174 us
  Pallas kernels  173 us (99%)
    pallas_call x1, Pallas kernels, shards(): pl.pallas_call(lambda *refs: fused_kernel(reps, *refs), out_shape=[half(P...  168 us
    pallas_call x1, Pallas kernels, shards(): pl.pallas_call(lambda *refs: widen_kernel(factor, *refs), out_shape=outs...  5.48 us

profile of v5, /device:TPU:0, one launch (start us, length us, event | category | flops | bytes accessed | tf_op | source)
XLA Modules:
  0.0 173.8 jit_solution(8060071025570867907)
XLA Ops:
  0.6 167.6 %fused_backward.1 = (bf16[8,32,2048]{2,1,0:T(8,128)(2,1)}, f32[1,2048]{1,0:T(1,128)}, bf16[384,2048]{1,0:T(8,128)(2,1)}, bf16[2048,384]{1,0:T(8,128)(2,1)}, bf16[2048,384]{1,0:T(8,128)(2,1)}) custom-call(bf16[8,32,2048]{2,1,0:T(8,128)(2,1)} %bitcast.5, bf16[8,32,2048]{2,1,0:T(8,128)(2,1)} %bitcast.6, f32[1,2048]{1,0:T(1,128)} %bitcast.8, ...), custom_call_target="tpu_custom_call" | custom-call | tf_op jit(solution)/shard_map/fused_backward/pallas_call | solution.py:603
  168.3 5.5 %widen.1 = (f32[384,2048]{1,0:T(8,128)}, f32[2048,384]{1,0:T(8,128)}, f32[2048,384]{1,0:T(8,128)}, bf16[256,2048]{1,0:T(8,128)(2,1)}, f32[1,2048]{1,0:T(1,128)}) custom-call(bf16[384,2048]{1,0:T(8,128)(2,1)} %get-tuple-element.15.refs_0_, bf16[2048,384]{1,0:T(8,128)(2,1)} %get-tuple-element.16.refs_1_, bf16[2048,384]{1,0:T(8,128)(2,1)} %get-tuple-element.17.refs_2_, ...), custom_call_target="tpu_custom_call" | custom-call | tf_op jit(solution)/shard_map/widen/pallas_call | solution.py:632
